TPU v7x, 32 devices: a whole 2x2x4 slice. The times are simulated.
32 devices in a mesh: ep: 8 (over z, x), tp: 4 (over y, core).
Axes of the slice: x: 2, y: 2, z: 4, core: 2. Of those that a mesh axis runs over, the one named last changes fastest.
Arguments:
- tokens: bfloat16 [1024, 2048], P('ep'), may hold values from -6 to 6
- chosen: int32 [8, 8, 7], P('ep'), may hold values from -1 to 127, as said below
- pick_weight: float32 [8, 8, 7], P('ep'), may hold values from 0.2 to 1
- gate_weight: bfloat16 [8, 2048, 4096], P('ep', None, 'tp'), may hold values from -0.125 to 0.125
- up_weight: bfloat16 [8, 2048, 4096], P('ep', None, 'tp'), may hold values from -0.125 to 0.125
- down_weight: bfloat16 [8, 4096, 2048], P('ep', 'tp'), may hold values from -0.09375 to 0.09375
Outputs:
- combined: bfloat16 [1024, 2048], P('ep', 'tp')
Inputs may be any that keep to these rules, and one draw needn't show every extreme that they name: `chosen`: within one group and one expert the named positions are distinct, and the filled slots come first. From each group every expert takes at least 3 tokens and at most 7; every expert takes exactly 7 tokens from some group, and exactly 40 tokens in all.
All inputs are finite; a program needn't handle non-finite values.
Results may differ from a plain program's by a relative error of at most 0.019.
Values may be sent and summed in bfloat16 or wider, within the bound.
A program may use at most 64 MiB of HBM per device.

v0:
```python
import jax
import jax.numpy as jnp
from jax import lax
from jax.sharding import PartitionSpec as P


def on_device(tokens, chosen, pick_weight, gate_weight, up_weight, down_weight):
    model_width = tokens.shape[1]
    experts = chosen.shape[1]
    slot_count = chosen.shape[2]
    chosen_ids = chosen[0]
    filled = chosen_ids >= 0
    safe_ids = jnp.where(filled, chosen_ids, 0).reshape(-1)
    picked = jnp.take(tokens, safe_ids, axis=0)
    picked = jnp.where(filled.reshape(-1, 1), picked, jnp.zeros((), tokens.dtype))
    picked = picked.reshape(experts, slot_count, model_width)
    received = lax.all_to_all(picked, "ep", split_axis=0, concat_axis=0, tiled=True)
    expert_rows = received.reshape(-1, model_width)
    gate_pre = jnp.dot(expert_rows, gate_weight[0], preferred_element_type=jnp.float32)
    up_pre = jnp.dot(expert_rows, up_weight[0], preferred_element_type=jnp.float32)
    hidden = (jax.nn.silu(gate_pre) * up_pre).astype(jnp.bfloat16)
    down_local = down_weight[0]
    summed = lax.psum_scatter(
        jnp.einsum("fd,rf->dr", down_local, hidden, preferred_element_type=jnp.float32).astype(
            jnp.bfloat16
        ),
        "tp",
        scatter_dimension=0,
        tiled=True,
    )
    returned = lax.all_to_all(summed, "ep", split_axis=1, concat_axis=1, tiled=True)
    weights = jnp.where(filled, pick_weight[0], jnp.zeros((), jnp.float32)).reshape(-1)
    positions = lax.iota(jnp.int32, tokens.shape[0])
    onehot = jnp.where(
        positions[:, None] == safe_ids[None, :], weights[None, :], jnp.zeros((), jnp.float32)
    )
    combined = jnp.einsum(
        "tk,wk->tw",
        onehot,
        returned.astype(jnp.float32),
        precision=lax.Precision.HIGHEST,
        preferred_element_type=jnp.float32,
    )
    return combined.astype(jnp.bfloat16)


def solution(mesh):
    return jax.shard_map(
        on_device,
        mesh=mesh,
        in_specs=(
            P("ep", None),
            P("ep", None, None),
            P("ep", None, None),
            P("ep", None, "tp"),
            P("ep", None, "tp"),
            P("ep", "tp", None),
        ),
        out_specs=P("ep", "tp"),
        check_vma=False,
    )
```

profile of v0, /device:TPU:0, one launch (start us, length us, event | category | flops | bytes accessed | tf_op | source)
XLA Modules:
  0.0 74.2 jit_solution(4793843722620870495)
XLA Ops:
  6.5 0.0 copy-start
  6.5 0.0 reduce-scatter.2.cloned.1.call-start
  6.5 0.8 %copy.11 = s32[1,8,7]{2,1,0:T(8,128)S(1)} copy(s32[1,8,7]{1,0,2:T(1,128)} %param.7) | data formatting | bytes 448 | tf_op args[1]
  7.4 0.1 squeeze.22
  7.5 0.1 copy-done
  7.6 0.7 gather_fusion
  8.3 0.1 gather.7
  8.4 0.1 select_select_fusion
  8.5 16.0 %all_to_all.17 = bf16[8,7,2048]{2,1,0:T(8,128)(2,1)S(1)} all-to-all(bf16[8,7,2048]{2,1,0:T(8,128)(2,1)S(1)} %select_select_fusion), channel_id=1, replica_groups=mesh['ep'=8,'tp'=4] {'ep'}, dimensions={0} | all-to-all | bytes 458752 | tf_op jit(solution)/shard_map/all_to_all | solution.py:17
  24.5 0.1 reshape.74
  24.6 3.0 %fusion.4 = f32[56,1024]{1,0:T(8,128)S(1)} fusion(bf16[56,2048]{1,0:T(8,128)(2,1)S(1)} %reshape.74, bf16[1,2048,1024]{2,1,0:T(8,128)(2,1)} %param.9), kind=kOutput, calls=%fused_computation.5 | convolution fusion | flops 234881024 | bytes 4653056 | tf_op jit(solution)/shard_map/dot_general | solution.py:19
  27.6 0.0 copy-start.1
  27.6 5.7 %fusion.9 = bf16[2048,56]{0,1:T(8,128)(2,1)} fusion(bf16[1,1024,2048]{2,1,0:T(8,128)(2,1)} %param.11, bf16[56,2048]{1,0:T(8,128)(2,1)S(1)} %reshape.74, bf16[1,2048,1024]{2,1,0:T(8,128)(2,1)} %param.10, f32[56,1024]{1,0:T(8,128)S(1)} %fusion.4), kind=kOutput, calls=%fused_computation.8 | convolution fusion | flops 470220800 | bytes 9076736 | tf_op jit(solution)/shard_map/fd,rf->dr/dot_general | solution.py:24
  33.4 0.0 reduce-scatter.2.cloned.1.call-update
  33.4 0.1 squeeze.19
  33.5 0.0 copy-done.1
  33.5 0.1 copy.12
  33.5 0.1 squeeze.20
  33.6 18.9 %reduce-scatter.2.cloned.1.call-done = bf16[512,56]{0,1:T(8,128)(2,1)} async-done(((bf16[2048,56]{0,1:T(8,128)(2,1)}), bf16[512,56]{0,1:T(8,128)(2,1)}) %reduce-scatter.2.cloned.1.call-update) | async-done | bytes 57360 | tf_op jit(solution)/shard_map/reduce_scatter | solution.py:23
  52.5 1.5 %all_to_all.12 = bf16[512,8,7]{0,2,1:T(8,128)(2,1)} reshape(bf16[512,56]{0,1:T(8,128)(2,1)} %reduce-scatter.2.cloned.1.call-done) | data formatting | bytes 114688 | tf_op jit(solution)/shard_map/all_to_all | solution.py:31
  54.0 5.5 %all-to-all-start.1 = ((bf16[512,8,7]{0,2,1:T(8,128)(2,1)}), bf16[512,8,7]{0,2,1:T(8,128)(2,1)S(1)}, u32[]{:S(2)}, u32[]{:S(2)}) async-start(bf16[512,8,7]{0,2,1:T(8,128)(2,1)} %all_to_all.12), calls=%async_computation.2 | async-start | bytes 131072 | tf_op jit(solution)/shard_map/all_to_all | solution.py:31
  59.5 6.9 %all-to-all-done.1 = bf16[512,8,7]{0,2,1:T(8,128)(2,1)S(1)} async-done(((bf16[512,8,7]{0,2,1:T(8,128)(2,1)}), bf16[512,8,7]{0,2,1:T(8,128)(2,1)S(1)}, u32[]{:S(2)}, u32[]{:S(2)}) %all-to-all-start.1) | async-done | bytes 57376 | tf_op jit(solution)/shard_map/all_to_all | solution.py:31
  66.4 0.9 %convolution_convert_fusion = bf16[128,512]{1,0:T(8,128)(2,1)} fusion(bf16[512,56]{0,1:T(8,128)(2,1)S(1)} %all_to_all.14, f32[56]{0:T(128)S(1)} %compare_select_fusion.3, s32[56]{0:T(128)S(1)} %compare_select_fusion.4), kind=kOutput, calls=%fused_computation.10 | convolution fusion | flops 44120064 | bytes 188864 | tf_op jit(solution)/shard_map/tk,wk->tw/dot_general | solution.py:37
  (6 shorter events, 0.1 us)
Async XLA Ops:
  6.5 1.1 %copy-start = (bf16[128,2048]{1,0:T(8,128)(2,1)S(1)}, bf16[128,2048]{1,0:T(8,128)(2,1)}, u32[]{:S(2)}) copy-start(bf16[128,2048]{1,0:T(8,128)(2,1)} %param.6) | copy-start | bytes 1572868
  6.5 46.0 %reduce-scatter.2.cloned.1.call-start = ((), (), s32[]{:S(2)}) async-start(), calls=%async_computation.3 | async-start | bytes 286720 | tf_op jit(solution)/shard_map/reduce_scatter | solution.py:23
  27.6 5.8 %copy-start.1 = (f32[1,8,7]{1,0,2:T(1,128)S(1)}, f32[1,8,7]{1,0,2:T(1,128)}, u32[]{:S(2)}) copy-start(f32[1,8,7]{1,0,2:T(1,128)} %param.8) | copy-start | bytes 676
  54.0 12.4 %all-to-all-start.1 = ((bf16[512,8,7]{0,2,1:T(8,128)(2,1)}), bf16[512,8,7]{0,2,1:T(8,128)(2,1)S(1)}, u32[]{:S(2)}, u32[]{:S(2)}) async-start(bf16[512,8,7]{0,2,1:T(8,128)(2,1)} %all_to_all.12), calls=%async_computation.2 | async-start | bytes 131072 | tf_op jit(solution)/shard_map/all_to_all | solution.py:31
Sparse Core Ops, SparseCore 0:
  33.5 18.9 reduce-scatter.1
where the time goes:
time: 74.5 us; the launch traced here: 74.2 us
  waiting for transfers between devices  25.8 us (35%)
  blocking collectives  16 us (21%)
  between operations  13.4 us (18%)
  matrix products  9.65 us (13%)
  starting transfers between devices  5.5 us (7%)
  local copies, waits for them, and re-layouts  3.66 us (5%)
    reduce_scatter x1, waiting for transfers between devices, on_device(): lax.psum_scatter(jnp.einsum('fd,rf->dr', down_local, hidden, preferred_el...  18.9 us
    all_to_all x1, blocking collectives, on_device(): lax.all_to_all(picked, 'ep', split_axis=0, concat_axis=0, tiled=True)  16 us
    all_to_all x1, waiting for transfers between devices, on_device(): lax.all_to_all(summed, 'ep', split_axis=1, concat_axis=1, tiled=True)  6.9 us
    dot_general x1, matrix products, on_device(): jnp.einsum('fd,rf->dr', down_local, hidden, preferred_element_type=jnp.fl...  5.72 us
    all_to_all x1, starting transfers between devices, on_device(): lax.all_to_all(summed, 'ep', split_axis=1, concat_axis=1, tiled=True)  5.5 us
    dot_general x1, matrix products, on_device(): jnp.dot(expert_rows, gate_weight[0], preferred_element_type=jnp.float32)  3.02 us
    all_to_all x2, local copies, waits for them, and re-layouts, on_device(): lax.all_to_all(summed, 'ep', split_axis=1, concat_axis=1, tiled=True)  1.51 us
  transfers between devices with their start and end apart: 2, of which 2 were waited for; matrix products, arithmetic and copies ran while one was open for 0% of the time, Pallas kernels for 0%

commit v1 on v0

--- a/solution.py
+++ b/solution.py
@@ -28,7 +28,10 @@
         scatter_dimension=0,
         tiled=True,
     )
-    returned = lax.all_to_all(summed, "ep", split_axis=1, concat_axis=1, tiled=True)
+    returned = jnp.concatenate(
+        lax.all_to_all(jnp.stack(jnp.split(summed, lax.axis_size("ep"), axis=1)), "ep", 0, 0),
+        axis=1,
+    )
     weights = jnp.where(filled, pick_weight[0], jnp.zeros((), jnp.float32)).reshape(-1)
     positions = lax.iota(jnp.int32, tokens.shape[0])
     onehot = jnp.where(

time: 74.5 us -> 84.2 us (1.13)
  local copies, waits for them, and re-layouts: 3.66 us -> 12.7 us
    unnamed x6 -> x13, local copies, waits for them, and re-layouts: 1.03 us -> 10.2 us
    all_to_all x2 -> x0, local copies, waits for them, and re-layouts: 1.51 us -> none  [on_device(): lax.all_to_all(summed, 'ep', split_axis=1, concat_axis=1, tiled=True)]
    another operation x0 -> x1, local copies, waits for them, and re-layouts: none -> 1.3 us  [on_device(): jnp.stack(jnp.split(summed, lax.axis_size('ep'), axis=1))]
where the time goes in v1:
time: 84.2 us; the launch traced here: 83.2 us
  waiting for transfers between devices  25.8 us (31%)
  blocking collectives  16 us (19%)
  between operations  13.5 us (16%)
  local copies, waits for them, and re-layouts  12.7 us (15%)
  matrix products  9.62 us (11%)
  starting transfers between devices  5.49 us (7%)
    reduce_scatter x1, waiting for transfers between devices, on_device(): lax.psum_scatter(jnp.einsum('fd,rf->dr', down_local, hidden, preferred_el...  18.9 us
    all_to_all x1, blocking collectives, on_device(): lax.all_to_all(picked, 'ep', split_axis=0, concat_axis=0, tiled=True)  16 us
    unnamed x13, local copies, waits for them, and re-layouts  10.2 us
    all_to_all x1, waiting for transfers between devices, on_device(): lax.all_to_all(jnp.stack(jnp.split(summed, lax.axis_size('ep'), axis=1)),...  6.9 us
    dot_general x1, matrix products, on_device(): jnp.einsum('fd,rf->dr', down_local, hidden, preferred_element_type=jnp.fl...  5.7 us
    all_to_all x1, starting transfers between devices, on_device(): lax.all_to_all(jnp.stack(jnp.split(summed, lax.axis_size('ep'), axis=1)),...  5.49 us
    dot_general x1, matrix products, on_device(): jnp.dot(expert_rows, gate_weight[0], preferred_element_type=jnp.float32)  3.01 us
  transfers between devices with their start and end apart: 2, of which 2 were waited for; matrix products, arithmetic and copies ran while one was open for 0% of the time, Pallas kernels for 0%

profile of v1, /device:TPU:0, one launch (start us, length us, event | category | flops | bytes accessed | tf_op | source)
XLA Modules:
  0.0 83.2 jit_solution(11330856904471773564)
XLA Ops:
  6.5 0.0 copy-start
  6.5 0.0 reduce-scatter.2.cloned.1.call-start
  6.5 0.8 copy.11
  7.4 0.1 squeeze.22
  7.5 0.1 copy-done
  7.6 0.7 gather_fusion
  8.3 0.1 gather.7
  8.4 0.1 select_select_fusion
  8.5 16.0 %all_to_all.10 = bf16[8,7,2048]{2,1,0:T(8,128)(2,1)S(1)} all-to-all(bf16[8,7,2048]{2,1,0:T(8,128)(2,1)S(1)} %select_select_fusion), channel_id=1, replica_groups=mesh['ep'=8,'tp'=4] {'ep'}, dimensions={0} | all-to-all | bytes 458752 | tf_op jit(solution)/shard_map/all_to_all | solution.py:17
  24.5 0.1 reshape.78
  24.6 3.0 %fusion.4 = f32[56,1024]{1,0:T(8,128)S(1)} fusion(bf16[56,2048]{1,0:T(8,128)(2,1)S(1)} %reshape.78, bf16[1,2048,1024]{2,1,0:T(8,128)(2,1)} %param.9), kind=kOutput, calls=%fused_computation.5 | convolution fusion | flops 234881024 | bytes 4653056 | tf_op jit(solution)/shard_map/dot_general | solution.py:19
  27.6 0.0 copy-start.1
  27.6 5.7 %fusion.9 = bf16[2048,56]{0,1:T(8,128)(2,1)} fusion(bf16[1,1024,2048]{2,1,0:T(8,128)(2,1)} %param.11, bf16[56,2048]{1,0:T(8,128)(2,1)S(1)} %reshape.78, bf16[1,2048,1024]{2,1,0:T(8,128)(2,1)} %param.10, f32[56,1024]{1,0:T(8,128)S(1)} %fusion.4), kind=kOutput, calls=%fused_computation.8 | convolution fusion | flops 470220800 | bytes 9076736 | tf_op jit(solution)/shard_map/fd,rf->dr/dot_general | solution.py:24
  33.3 0.0 reduce-scatter.2.cloned.1.call-update
  33.4 0.1 squeeze.19
  33.4 0.0 copy-done.1
  33.4 0.1 copy.12
  33.5 0.1 squeeze.20
  33.6 18.9 %reduce-scatter.2.cloned.1.call-done = bf16[512,56]{0,1:T(8,128)(2,1)} async-done(((bf16[2048,56]{0,1:T(8,128)(2,1)}), bf16[512,56]{0,1:T(8,128)(2,1)}) %reduce-scatter.2.cloned.1.call-update) | async-done | bytes 57360 | tf_op jit(solution)/shard_map/reduce_scatter | solution.py:23
  52.5 1.3 %constant_dynamic-update-slice_fusion.7 = bf16[8,512,7]{1,2,0:T(8,128)(2,1)} fusion(bf16[512,56]{0,1:T(8,128)(2,1)} %reduce-scatter.2.cloned.1.call-done), kind=kLoop, calls=%fused_computation.31 | loop fusion | bytes 15360
  53.8 1.3 %constant_dynamic-update-slice_fusion.6 = bf16[8,512,7]{1,2,0:T(8,128)(2,1)} fusion(bf16[8,512,7]{1,2,0:T(8,128)(2,1)} %constant_dynamic-update-slice_fusion.7, bf16[512,56]{0,1:T(8,128)(2,1)} %reduce-scatter.2.cloned.1.call-done), kind=kLoop, calls=%fused_computation.30 | loop fusion | bytes 16384
  55.1 1.3 %constant_dynamic-update-slice_fusion.5 = bf16[8,512,7]{1,2,0:T(8,128)(2,1)} fusion(bf16[8,512,7]{1,2,0:T(8,128)(2,1)} %constant_dynamic-update-slice_fusion.6, bf16[512,56]{0,1:T(8,128)(2,1)} %reduce-scatter.2.cloned.1.call-done), kind=kLoop, calls=%fused_computation.29 | loop fusion | bytes 16384
  56.4 1.3 %constant_dynamic-update-slice_fusion.4 = bf16[8,512,7]{1,2,0:T(8,128)(2,1)} fusion(bf16[8,512,7]{1,2,0:T(8,128)(2,1)} %constant_dynamic-update-slice_fusion.5, bf16[512,56]{0,1:T(8,128)(2,1)} %reduce-scatter.2.cloned.1.call-done), kind=kLoop, calls=%fused_computation.28 | loop fusion | bytes 16384
  57.7 1.3 %constant_dynamic-update-slice_fusion.3 = bf16[8,512,7]{1,2,0:T(8,128)(2,1)} fusion(bf16[8,512,7]{1,2,0:T(8,128)(2,1)} %constant_dynamic-update-slice_fusion.4, bf16[512,56]{0,1:T(8,128)(2,1)} %reduce-scatter.2.cloned.1.call-done), kind=kLoop, calls=%fused_computation.27 | loop fusion | bytes 16384
  59.0 1.3 %constant_dynamic-update-slice_fusion.2 = bf16[8,512,7]{1,2,0:T(8,128)(2,1)} fusion(bf16[8,512,7]{1,2,0:T(8,128)(2,1)} %constant_dynamic-update-slice_fusion.3, bf16[512,56]{0,1:T(8,128)(2,1)} %reduce-scatter.2.cloned.1.call-done), kind=kLoop, calls=%fused_computation.26 | loop fusion | bytes 16384
  60.4 1.3 %constant_dynamic-update-slice_fusion.1 = bf16[8,512,7]{1,2,0:T(8,128)(2,1)} fusion(bf16[8,512,7]{1,2,0:T(8,128)(2,1)} %constant_dynamic-update-slice_fusion.2, bf16[512,56]{0,1:T(8,128)(2,1)} %reduce-scatter.2.cloned.1.call-done), kind=kLoop, calls=%fused_computation.25 | loop fusion | bytes 16384
  61.7 1.3 %constant_dynamic-update-slice_fusion = bf16[8,512,7]{1,2,0:T(8,128)(2,1)} fusion(bf16[8,512,7]{1,2,0:T(8,128)(2,1)} %constant_dynamic-update-slice_fusion.1, bf16[512,56]{0,1:T(8,128)(2,1)} %reduce-scatter.2.cloned.1.call-done), kind=kLoop, calls=%fused_computation.24 | loop fusion | bytes 16384 | tf_op jit(solution)/shard_map/stack | solution.py:32
  63.0 5.5 %all-to-all-start.1 = ((bf16[8,512,7]{1,2,0:T(8,128)(2,1)}), bf16[8,512,7]{1,2,0:T(8,128)(2,1)S(1)}, u32[]{:S(2)}, u32[]{:S(2)}) async-start(bf16[8,512,7]{1,2,0:T(8,128)(2,1)} %constant_dynamic-update-slice_fusion), calls=%async_computation.2 | async-start | bytes 131072 | tf_op jit(solution)/shard_map/all_to_all | solution.py:32
  68.5 6.9 %all-to-all-done.1 = bf16[8,512,7]{1,2,0:T(8,128)(2,1)S(1)} async-done(((bf16[8,512,7]{1,2,0:T(8,128)(2,1)}), bf16[8,512,7]{1,2,0:T(8,128)(2,1)S(1)}, u32[]{:S(2)}, u32[]{:S(2)}) %all-to-all-start.1) | async-done | bytes 57376 | tf_op jit(solution)/shard_map/all_to_all | solution.py:32
  75.4 0.9 %convolution_convert_fusion = bf16[128,512]{1,0:T(8,128)(2,1)} fusion(bf16[512,56]{0,1:T(8,128)(2,1)S(1)} %reshape.80, f32[56]{0:T(128)S(1)} %compare_select_fusion.3, s32[56]{0:T(128)S(1)} %compare_select_fusion.4), kind=kOutput, calls=%fused_computation.10 | convolution fusion | flops 44120064 | bytes 188864 | tf_op jit(solution)/shard_map/tk,wk->tw/dot_general | solution.py:40
  (6 shorter events, 0.1 us)
Async XLA Ops:
  6.5 1.1 %copy-start = (bf16[128,2048]{1,0:T(8,128)(2,1)S(1)}, bf16[128,2048]{1,0:T(8,128)(2,1)}, u32[]{:S(2)}) copy-start(bf16[128,2048]{1,0:T(8,128)(2,1)} %param.6) | copy-start | bytes 1572868
  6.5 45.9 %reduce-scatter.2.cloned.1.call-start = ((), (), s32[]{:S(2)}) async-start(), calls=%async_computation.3 | async-start | bytes 286720 | tf_op jit(solution)/shard_map/reduce_scatter | solution.py:23
  27.6 5.8 %copy-start.1 = (f32[1,8,7]{1,0,2:T(1,128)S(1)}, f32[1,8,7]{1,0,2:T(1,128)}, u32[]{:S(2)}) copy-start(f32[1,8,7]{1,0,2:T(1,128)} %param.8) | copy-start | bytes 676
  63.0 12.4 %all-to-all-start.1 = ((bf16[8,512,7]{1,2,0:T(8,128)(2,1)}), bf16[8,512,7]{1,2,0:T(8,128)(2,1)S(1)}, u32[]{:S(2)}, u32[]{:S(2)}) async-start(bf16[8,512,7]{1,2,0:T(8,128)(2,1)} %constant_dynamic-update-slice_fusion), calls=%async_computation.2 | async-start | bytes 131072 | tf_op jit(solution)/shard_map/all_to_all | solution.py:32
Sparse Core Ops, SparseCore 0:
  33.5 18.9 reduce-scatter.1
